TPU v7x, 512 devices: a whole 4x4x16 slice. The times are simulated.
512 devices in a mesh: fs: 64 (over z, y), tp: 8 (over x, core).
Axes of the slice: x: 4, y: 4, z: 16, core: 2. Of those that a mesh axis runs over, the one named last changes fastest.
Arguments:
- tokens: bfloat16 [32768, 2048], P('fs', 'tp'), may hold values from -24 to 24
- u_weight: bfloat16 [2048, 1024], P('fs', 'tp'), may hold values from -0.125 to 0.125
- v_weight: bfloat16 [2048, 1024], P('fs', 'tp'), may hold values from -0.125 to 0.125
- sg_gain: float32 [1024], P('tp'), may hold values from 0.1 to 1.9
- spatial_weight: bfloat16 [8, 128, 128], P('tp'), may hold values from -0.5 to 0.5
- spatial_bias: float32 [8, 128], P('tp'), may hold values from 0.1 to 1.9
- out_weight: bfloat16 [1024, 2048], P('tp', 'fs'), may hold values from -0.1875 to 0.1875
- gain_one: float32 [2048], P('tp'), may hold values from 0.1 to 1.9
- gate_weight: bfloat16 [2048, 5632], P('fs', 'tp'), may hold values from -0.125 to 0.125
- up_weight: bfloat16 [2048, 5632], P('fs', 'tp'), may hold values from -0.125 to 0.125
- down_weight: bfloat16 [5632, 2048], P('tp', 'fs'), may hold values from -0.078125 to 0.078125
- gain_two: float32 [2048], P('tp'), may hold values from 0.1 to 1.9
Outputs:
- layer_out: bfloat16 [32768, 2048], P('fs', 'tp')
All inputs are finite; a program needn't handle non-finite values.
Results may differ from a plain program's by a relative error of at most 0.014.
Values may be sent and summed in bfloat16 or wider, within the bound.
No kernel may reach another device: no remote copies, remote signals or barrier semaphores. Data moves between devices by JAX's collectives and lax.ppermute only.
A program may use at most 64 MiB of HBM per device.

v0:
```python
import jax
import jax.numpy as jnp
from jax import lax
from jax.experimental import pallas as pl
from jax.experimental.pallas import tpu as pltpu
from jax.sharding import Mesh
from jax.sharding import PartitionSpec as P

FS = ("z", "y")
TP = ("x", "c")

EPS = 1e-05
ALPHA = 2.0**0.25
BF16 = jnp.bfloat16
F32 = jnp.float32
ACROSS = (((1,), (1,)), ((), ()))


def sent_to_all(value, axis):
    copies = jnp.broadcast_to(value, (lax.axis_size(axis), *value.shape))
    return lax.all_to_all(copies, axis, split_axis=0, concat_axis=0, tiled=True)


def to_partner(value):
    return lax.ppermute(value, "c", [(0, 1), (1, 0)])


def row_norm(vals, gain):
    count = vals.shape[1]
    mean = jnp.sum(vals, axis=1, keepdims=True) / count
    square = jnp.sum(vals * vals, axis=1, keepdims=True) / count
    return (vals - mean) * lax.rsqrt(square - mean * mean + EPS) * gain


def in_vmem(value):
    return pltpu.with_memory_space_constraint(value, pltpu.VMEM)


def in_hbm(value):
    return pltpu.with_memory_space_constraint(value, pltpu.HBM)


def whole_vmem():
    return pl.BlockSpec(memory_space=pltpu.VMEM)


def last_norm(pieces, base, gain, parts):
    peers, rows, width = pieces.shape

    def body(pieces_ref, base_ref, gain_ref, out_ref):
        added = pieces_ref[0].astype(F32)
        for k in range(1, peers):
            added = added + pieces_ref[k].astype(F32)
        vals = ALPHA * base_ref[...].astype(F32) + added.astype(BF16).astype(F32)
        done = row_norm(vals, gain_ref[...]).astype(BF16)
        for k in range(parts):
            out_ref[k] = done[:, k * (width // parts) : (k + 1) * (width // parts)]

    return pl.pallas_call(
        body,
        out_shape=pltpu.VMEM((parts, rows, width // parts), BF16),
        in_specs=[whole_vmem()] * 3,
        out_specs=whole_vmem(),
        name="last_norm",
    )(in_vmem(pieces), in_vmem(base), gain.reshape(1, width))


def branches(blocks, gates, gains):
    parts, rows, feats = blocks.shape
    ys, deep, columns = gates.shape
    width = parts * feats
    half = columns // 2
    depth = 32

    def body(blocks_ref, gates_ref, gains_ref, gated_ref, valued_ref, sums_ref, left, right, sems):
        copies = []
        for k in range(parts):
            copies.append(pltpu.make_async_copy(blocks_ref.at[k], left.at[:, pl.ds(k * feats, feats)], sems.at[k]))
            copies[k].start()
        for z in range(deep // depth):
            for y in range(ys):
                at = (z * ys + y) * depth
                right[at : at + depth] = gates_ref[y, z * depth : (z + 1) * depth]
        for c in copies:
            c.wait()
        both = jnp.dot(left[...], right[...], preferred_element_type=F32)
        gated_ref[...] = jax.nn.gelu(both[:, :half])
        valued = jax.nn.gelu(both[:, half:])
        valued_ref[...] = valued
        turned = valued.T
        total = jnp.sum(turned, axis=0, keepdims=True)
        squares = jnp.sum(turned * turned, axis=0, keepdims=True)
        for k in range(parts):
            sums_ref[k, 0:1] = total
            sums_ref[k, 1:2] = squares
            sums_ref[k, 2:3] = gains_ref[...]
            sums_ref[k, 3:4] = gains_ref[...]

    return pl.pallas_call(
        body,
        out_shape=(
            pltpu.VMEM((rows, half), F32),
            pltpu.VMEM((rows, half), F32),
            pltpu.VMEM((parts, 4, rows), F32),
        ),
        in_specs=[pl.BlockSpec(memory_space=pltpu.HBM), whole_vmem(), whole_vmem()],
        out_specs=(whole_vmem(),) * 3,
        scratch_shapes=[
            pltpu.VMEM((rows, width), BF16),
            pltpu.VMEM((width, columns), BF16),
            pltpu.SemaphoreType.DMA((parts,)),
        ],
        compiler_params=pltpu.CompilerParams(vmem_limit_bytes=24 << 20),
        cost_estimate=pl.CostEstimate(flops=2 * rows * width * columns, bytes_accessed=4 << 20, transcendentals=2 * rows * columns),
        name="branches",
    )(in_hbm(blocks), in_vmem(gates), gains)


def gated_copies(known, gated, valued, gain, weight, bias, copies):
    parts, _, rows = known.shape
    channels = gated.shape[1]
    block = weight.shape[1]
    count = parts * channels

    def body(known_ref, gated_ref, valued_ref, gain_ref, weight_ref, bias_ref, out_ref):
        sums = known_ref[0]
        for k in range(1, parts):
            sums = sums + known_ref[k]
        mean = sums[0:1] / count
        square = sums[1:2] / count
        scale = lax.rsqrt(square - mean * mean + EPS)
        mean = jnp.broadcast_to(mean, (channels, rows)).T
        scale = jnp.broadcast_to(scale, (channels, rows)).T
        normed = ((valued_ref[...] - mean) * scale * gain_ref[...]).astype(BF16)
        row = lax.broadcasted_iota(jnp.int32, (block, block), 0)
        column = lax.broadcasted_iota(jnp.int32, (block, block), 1)
        masked = jnp.where(row >= column, weight_ref[0].astype(F32), 0.0).astype(BF16)
        offset = jnp.broadcast_to(bias_ref[...], (channels, block)).T
        for n in range(rows // block):
            at = slice(n * block, (n + 1) * block)
            mixed = jnp.dot(masked, normed[at], preferred_element_type=F32) + offset
            done = (gated_ref[at] * mixed).astype(BF16)
            for k in range(copies):
                out_ref[k, at] = done

    return pl.pallas_call(
        body,
        out_shape=pltpu.VMEM((copies, rows, channels), BF16),
        in_specs=[whole_vmem()] * 6,
        out_specs=whole_vmem(),
        compiler_params=pltpu.CompilerParams(vmem_limit_bytes=12 << 20),
        cost_estimate=pl.CostEstimate(flops=2 * rows * block * channels, bytes_accessed=2 << 20, transcendentals=rows),
        name="gated_copies",
    )(in_vmem(known), in_vmem(gated), in_vmem(valued), gain.reshape(1, channels), weight, bias)


def projected(place, gated, pieces):
    chips, rows, channels = gated.shape
    peers = len(pieces)
    depth = 32
    zs = pieces[0].shape[0] // chips // depth
    width = zs * peers * depth
    steps = 8
    deep = zs // steps
    span = width // steps
    ahead = 3

    def body(place_ref, gated_ref, *rest):
        pieces = rest[:peers]
        out_ref, weights, left, sems = rest[peers:]
        y = place_ref[2]
        copies = []
        for j in range(steps):
            at_z = pl.ds(j * deep, deep)
            some = []
            for n in range(peers):
                at_y = lax.rem(y + peers - n, peers)
                some.append(pltpu.make_async_copy(pieces[n].at[:, at_z], weights.at[:, at_z, at_y], sems.at[j, n]))
            copies.append(some)
        for some in copies[:ahead]:
            for c in some:
                c.start()
        for k in range(chips):
            left[:, k * channels : (k + 1) * channels] = gated_ref[k]
        for j in range(steps):
            for c in copies[j]:
                c.wait()
            if j + ahead < steps:
                for c in copies[j + ahead]:
                    c.start()
            right = [weights[k, j * deep : (j + 1) * deep].reshape(span, channels) for k in range(chips)]
            right = jnp.concatenate(right, axis=1)
            part = lax.dot_general(left[...], right, ACROSS, preferred_element_type=F32)
            out_ref[:, j * span : (j + 1) * span] = part.astype(BF16)

    given = [p.reshape(chips, zs, depth, channels) for p in pieces]
    anywhere = pl.BlockSpec(memory_space=pl.ANY)
    return pl.pallas_call(
        body,
        out_shape=jax.ShapeDtypeStruct((rows, width), BF16),
        in_specs=[pl.BlockSpec(memory_space=pltpu.SMEM), whole_vmem()] + [anywhere] * peers,
        out_specs=whole_vmem(),
        scratch_shapes=[
            pltpu.VMEM((chips, zs, peers, depth, channels), BF16),
            pltpu.VMEM((rows, chips * channels), BF16),
            pltpu.SemaphoreType.DMA((steps, peers)),
        ],
        cost_estimate=pl.CostEstimate(flops=2 * rows * width * chips * channels, bytes_accessed=6 << 20, transcendentals=0),
        name="projected",
    )(in_hbm(place), in_vmem(gated), *given)


def mixer(place, own, other, blocks, gain, ffw, ff):
    rows, width = own.shape
    parts, _, feats = blocks.shape
    chips = parts // 2
    half = rows // 2
    few = rows // parts
    edges = [0, 384, 768, 1152, 2 * ff, 3 * ff]
    spans = [e - b for b, e in zip(edges, edges[1:])]
    chunks = len(spans)
    ahead = 3
    step = 256
    lanes = 128

    def body(place_ref, own_ref, other_ref, blocks_ref, gain_ref, ffw_ref, mine_ref, hidden_ref, give_ref, *rest):
        weights = rest[:chunks]
        base, low, vals, left, acc, in_sems, sems = rest[chunks:]
        core = place_ref[0]
        me = place_ref[1]
        inputs = []
        for j in range(parts):
            at = pl.ds(j * feats, feats)
            inputs.append(
                [
                    pltpu.make_async_copy(own_ref.at[:, at], low.at[j], in_sems.at[j, 0]),
                    pltpu.make_async_copy(blocks_ref.at[j], base.at[j], in_sems.at[j, 1]),
                ]
            )
            for c in inputs[j]:
                c.start()
        copies = []
        for n in range(chunks):
            at = pl.ds(edges[n], spans[n])
            copies.append(pltpu.make_async_copy(ffw_ref.at[:, at], weights[n], sems.at[n]))
        for c in copies[:ahead]:
            c.start()
        total = jnp.zeros((rows, lanes), F32)
        squares = jnp.zeros((rows, lanes), F32)
        for j in range(parts):
            for c in inputs[j]:
                c.wait()
            for b in range(0, feats, lanes):
                high = other_ref[:, j * feats + b : j * feats + b + lanes]
                mix = (low[j, :, b : b + lanes].astype(F32) + high.astype(F32)).astype(BF16)
                these = ALPHA * base[j, :, b : b + lanes].astype(F32) + mix.astype(F32)
                vals[j, :, b : b + lanes] = these
                total += these
                squares += these * these
        mean = jnp.sum(total, axis=1, keepdims=True) / width
        scale = lax.rsqrt(jnp.sum(squares, axis=1, keepdims=True) / width - mean * mean + EPS)
        for j in range(parts):
            at = slice(j * feats, (j + 1) * feats)
            left[:, at] = ((vals[j] - mean) * scale * gain_ref[:, at]).astype(BF16)
        mine_ref[...] = left[pl.ds(pl.multiple_of(me * few, few), few), :]
        for n in range(chunks - 1):
            copies[n].wait()
            if n + ahead < chunks:
                copies[n + ahead].start()
            acc[:, edges[n] : edges[n + 1]] = jnp.dot(left[...], weights[n][...], preferred_element_type=F32)
        gate = acc[:, :ff]
        hidden = (gate * lax.logistic(gate) * acc[:, ff:]).astype(BF16)
        copies[-1].wait()

        def rows_of(which):
            return jnp.concatenate([hidden[(2 * x + which) * few : (2 * x + which + 1) * few] for x in range(chips)], axis=0)

        def out(keep_core):
            hidden_ref[...] = rows_of(keep_core)
            given = rows_of(1 - keep_core)
            for b in range(0, width, step):
                done = lax.dot_general(given, weights[-1][b : b + step], ACROSS, preferred_element_type=F32)
                give_ref[:, b : b + step] = done.astype(BF16)

        @pl.when(core == 0)
        def _():
            out(0)

        @pl.when(core == 1)
        def _():
            out(1)

    anywhere = pl.BlockSpec(memory_space=pltpu.HBM)
    return pl.pallas_call(
        body,
        out_shape=(
            pltpu.VMEM((few, width), BF16),
            pltpu.VMEM((half, ff), BF16),
            pltpu.VMEM((half, width), BF16),
        ),
        in_specs=[pl.BlockSpec(memory_space=pltpu.SMEM), anywhere, whole_vmem(), anywhere, whole_vmem(), anywhere],
        out_specs=(whole_vmem(),) * 3,
        scratch_shapes=[
            *(pltpu.VMEM((width, n), BF16) for n in spans),
            pltpu.VMEM((parts, rows, feats), BF16),
            pltpu.VMEM((parts, rows, feats), BF16),
            pltpu.VMEM((parts, rows, feats), F32),
            pltpu.VMEM((rows, width), BF16),
            pltpu.VMEM((rows, 2 * ff), F32),
            pltpu.SemaphoreType.DMA((parts, 2)),
            pltpu.SemaphoreType.DMA((chunks,)),
        ],
        cost_estimate=pl.CostEstimate(flops=6 * rows * width * ff, bytes_accessed=18 << 20, transcendentals=rows * ff),
        name="mixer",
        compiler_params=pltpu.CompilerParams(vmem_limit_bytes=40 << 20),
    )(in_hbm(place), in_hbm(own), in_vmem(other), in_hbm(blocks), gain.reshape(1, width), in_hbm(ffw))


def kept(hidden, ffw):
    half, ff = hidden.shape
    width = ffw.shape[0]
    steps = 4
    span = width // steps

    def body(hidden_ref, ffw_ref, out_ref, weights, sems):
        copies = []
        for n in range(steps):
            at = pl.ds(n * span, span)
            copies.append(pltpu.make_async_copy(ffw_ref.at[at, pl.ds(2 * ff, ff)], weights.at[at], sems.at[n]))
            copies[n].start()
        for n in range(steps):
            copies[n].wait()
            at = slice(n * span, (n + 1) * span)
            done = lax.dot_general(hidden_ref[...], weights[at], ACROSS, preferred_element_type=F32)
            out_ref[:, at] = done.astype(BF16)

    return pl.pallas_call(
        body,
        out_shape=pltpu.VMEM((half, width), BF16),
        in_specs=[whole_vmem(), pl.BlockSpec(memory_space=pltpu.HBM)],
        out_specs=whole_vmem(),
        scratch_shapes=[pltpu.VMEM((width, ff), BF16), pltpu.SemaphoreType.DMA((steps,))],
        compiler_params=pltpu.CompilerParams(vmem_limit_bytes=12 << 20),
        cost_estimate=pl.CostEstimate(flops=2 * half * width * ff, bytes_accessed=4 << 20, transcendentals=0),
        name="kept",
    )(in_vmem(hidden), in_hbm(ffw))


def from_each(value, axis):
    size = lax.axis_size(axis)
    return [value] + [lax.ppermute(value, axis, [(i, (i + k) % size) for i in range(size)]) for k in range(1, size)]


def on_device(
    tokens,
    u_weight,
    v_weight,
    sg_gain,
    spatial_weight,
    spatial_bias,
    out_weight,
    gain_one,
    gate_weight,
    up_weight,
    down_weight,
    gain_two,
):
    core = lax.axis_index("c")
    chips = lax.axis_size("x")
    parts = chips * lax.axis_size("c")
    rows, feats = tokens.shape
    width = feats * parts
    sg = u_weight.shape[1]
    own_rows = rows // parts

    blocks = sent_to_all(tokens, TP)

    ffw = sent_to_all(jnp.concatenate([gate_weight, up_weight, down_weight.T], axis=1), "y")
    ffw = ffw.reshape(-1, ffw.shape[2])
    ffw = lax.all_gather(ffw, "z", axis=0, tiled=True)

    small = jnp.concatenate([u_weight, v_weight, out_weight.T], axis=1)
    small = lax.all_gather(small, "z", axis=0, tiled=True)
    gates = sent_to_all(small[:, : 2 * sg], "y")
    out_x = lax.all_gather(small[:, 2 * sg :], "x", axis=0, tiled=True)
    out_rows = from_each(out_x, "y")

    gains = jnp.concatenate([gain_one, gain_two]).reshape(1, rows)
    gated, valued, sums = branches(blocks, gates, gains)
    known = lax.all_to_all(sums, TP, 0, 0, tiled=True)
    gains = known[:, 2].reshape(parts, 2, feats)
    gain_1 = gains[:, 0].reshape(width)
    gain_2 = gains[:, 1].reshape(width)
    copies = gated_copies(known, gated, valued, sg_gain, spatial_weight, spatial_bias, chips)
    together = lax.all_to_all(copies, "x", 0, 0, tiled=True)
    place = jnp.stack([core, lax.axis_index(TP), lax.axis_index("y")]).astype(jnp.int32)
    own = projected(place, together, out_rows)
    mine, hidden, give = mixer(place, own, to_partner(own), blocks, gain_1, ffw, gate_weight.shape[1])
    keep = kept(hidden, ffw)
    pair = (keep.astype(F32) + to_partner(give).astype(F32)).astype(BF16)
    pieces = lax.all_to_all(pair.reshape(chips, own_rows, width), "x", 0, 0, tiled=True)
    last = last_norm(pieces, mine, gain_2, parts)
    return lax.all_to_all(last, TP, 0, 0, tiled=True).reshape(rows, feats)


def solution(mesh):
    tp = mesh.shape["tp"]
    finer = Mesh(mesh.devices.reshape(16, 4, tp // 2, 2), ("z", "y", "x", "c"))
    return jax.shard_map(
        on_device,
        mesh=finer,
        in_specs=(
            P(FS, TP),
            P(FS, TP),
            P(FS, TP),
            P(TP),
            P(TP, None, None),
            P(TP, None),
            P(TP, FS),
            P(TP),
            P(FS, TP),
            P(FS, TP),
            P(TP, FS),
            P(TP),
        ),
        out_specs=P(FS, TP),
        check_vma=False,
    )
```

profile of v0, /device:TPU:1, one launch (start us, length us, event | category | flops | bytes accessed | tf_op | source)
XLA Modules:
  0.0 220.2 jit_solution(12216790775809021771)
XLA Ops:
  7.6 12.0 %all_to_all.35 = bf16[4,32,2112]{2,1,0:T(8,128)(2,1)} all-to-all(bf16[4,32,2112]{2,1,0:T(8,128)(2,1)S(1)} %broadcast_in_dim.11), channel_id=1, replica_groups=mesh['z'=16,'y'=4,'x'=4,'c'=2] {'y'}, dimensions={0} | all-to-all | bytes 1081344 | tf_op jit(solution)/shard_map/all_to_all | solution.py:21
  19.7 34.5 %all_gather.9 = bf16[512,384]{1,0:T(8,128)(2,1)S(1)} all-gather(bf16[32,384]{1,0:T(8,128)(2,1)S(1)} %pad_maximum_fusion), channel_id=1, replica_groups=mesh['z'=16,'y'=4,'x'=4,'c'=2] {'z'}, dimensions={0}, use_global_device_ids=true | all-gather | bytes 417792 | tf_op jit(solution)/shard_map/all_gather | solution.py:383
  55.0 12.3 %all_to_all.36.gates_ref = bf16[4,512,256]{2,1,0:T(8,128)(2,1)S(1)} all-to-all(bf16[4,512,256]{2,1,0:T(8,128)(2,1)S(1)} %broadcast_in_dim.10), channel_id=1, replica_groups=mesh['z'=16,'y'=4,'x'=4,'c'=2] {'y'}, dimensions={0} | all-to-all | bytes 2097152 | tf_op jit(solution)/shard_map/all_to_all | solution.py:21
  67.3 1.5 broadcast_in_dim.9
  68.7 14.5 %all-to-all-start = ((bf16[8,512,256]{2,1,0:T(8,128)(2,1)}), bf16[8,512,256]{2,1,0:T(8,128)(2,1)S(1)}, u32[]{:S(2)}, u32[]{:S(2)}) async-start(bf16[8,512,256]{2,1,0:T(8,128)(2,1)} %broadcast_in_dim.9), calls=%async_computation | async-start | bytes 4194304 | tf_op jit(solution)/shard_map/all_to_all | solution.py:21
  83.2 33.8 %all_gather.10 = bf16[2048,128]{1,0:T(8,128)(2,1)} all-gather(bf16[512,128]{1,0:T(8,128)(2,1)S(1)} %slice-done), channel_id=1, replica_groups=mesh['z'=16,'y'=4,'x'=4,'c'=2] {'x'}, dimensions={0}, use_global_device_ids=true | all-gather | bytes 655360 | tf_op jit(solution)/shard_map/all_gather | solution.py:385
  117.0 2.8 %collective-permute-start.2 = (bf16[2048,128]{1,0:T(8,128)(2,1)}, bf16[2048,128]{1,0:T(8,128)(2,1)}, u32[]{:S(2)}, u32[]{:S(2)}) collective-permute-start(bf16[2048,128]{1,0:T(8,128)(2,1)} %all_gather.10), channel_id=1, source_target_pairs={{0,24},{8,0},{16,8},{24,16},{1,25},{9,1},{17,9},{25,17},{2,26},{10... | collective-permute-start | bytes 1572872 | tf_op jit(solution)/shard_map/ppermute | solution.py:351
  119.8 3.1 %collective-permute-start.1 = (bf16[2048,128]{1,0:T(8,128)(2,1)}, bf16[2048,128]{1,0:T(8,128)(2,1)}, u32[]{:S(2)}, u32[]{:S(2)}) collective-permute-start(bf16[2048,128]{1,0:T(8,128)(2,1)} %all_gather.10), channel_id=1, source_target_pairs={{0,16},{8,24},{16,0},{24,8},{1,17},{9,25},{17,1},{25,9},{2,18},{10... | collective-permute-start | bytes 1572872 | tf_op jit(solution)/shard_map/ppermute | solution.py:351
  122.9 1.9 collective-permute-start
  124.9 1.3 copy-done.3
  126.2 2.5 %branches.1 = (f32[512,128]{1,0:T(8,128)S(1)}, f32[512,128]{1,0:T(8,128)S(1)}, f32[8,4,512]{2,1,0:T(4,128)S(1)}) custom-call(bf16[8,512,256]{2,1,0:T(8,128)(2,1)} %copy-done.3, bf16[4,512,256]{2,1,0:T(8,128)(2,1)S(1)} %all_to_all.36.gates_ref, f32[1,512]{1,0:T(1,128)S(1)} %bitcast.18), custom_call_target="tpu_custom_call" | custom-call | flops 536870912 | bytes 4194304 | tf_op jit(solution)/shard_map/branches/pallas_call | solution.py:99
  128.6 10.3 %all_to_all.37.known_ref = f32[8,4,512]{2,1,0:T(4,128)S(1)} all-to-all(f32[8,4,512]{2,1,0:T(4,128)S(1)} %get-tuple-element.11), channel_id=1, replica_groups=mesh['z'=16,'y'=4,'x'=4,'c'=2] {'x','c'}, dimensions={0} | all-to-all | bytes 131072 | tf_op jit(solution)/shard_map/all_to_all | solution.py:390
  138.9 1.2 gated_copies.1
  140.1 3.5 %all-to-all-start.3 = ((bf16[4,512,128]{2,1,0:T(8,128)(2,1)}), bf16[4,512,128]{2,1,0:T(8,128)(2,1)S(1)}, u32[]{:S(2)}, u32[]{:S(2)}) async-start(bf16[4,512,128]{2,1,0:T(8,128)(2,1)} %gated_copies.1), calls=%async_computation.3 | async-start | bytes 1048576 | tf_op jit(solution)/shard_map/all_to_all | solution.py:395
  144.2 4.4 %collective-permute-done = bf16[2048,128]{1,0:T(8,128)(2,1)} collective-permute-done((bf16[2048,128]{1,0:T(8,128)(2,1)}, bf16[2048,128]{1,0:T(8,128)(2,1)}, u32[]{:S(2)}, u32[]{:S(2)}) %collective-permute-start) | collective-permute-done | bytes 524320 | tf_op jit(solution)/shard_map/ppermute | solution.py:351
  148.6 4.2 %all-to-all-done.3.gated_ref = bf16[4,512,128]{2,1,0:T(8,128)(2,1)S(1)} async-done(((bf16[4,512,128]{2,1,0:T(8,128)(2,1)}), bf16[4,512,128]{2,1,0:T(8,128)(2,1)S(1)}, u32[]{:S(2)}, u32[]{:S(2)}) %all-to-all-start.3) | async-done | bytes 524320 | tf_op jit(solution)/shard_map/all_to_all | solution.py:395
  152.7 7.0 %projected.1.own_ref = bf16[512,2048]{1,0:T(8,128)(2,1)} custom-call(s32[3]{0:T(128)} %pad_add_fusion.place_ref, bf16[4,512,128]{2,1,0:T(8,128)(2,1)S(1)} %all-to-all-done.3.gated_ref, bf16[4,16,32,128]{3,2,1,0:T(8,128)(2,1)} %bitcast.6.rest_0_, bf16[4,16,32,128]{3,2,1,0:T(8,128)(2,1)} %bitcast.7.rest_1_, bf16[4,16,32,128]{3,2,1,0:T(8,128)(2,1)} %bitcast.8.rest_2_, ...), custom_call_target="tpu_custom_call" | custom-call | flops 1073741824 | bytes 6291456 | tf_op jit(solution)/shard_map/projected/pallas_call | solution.py:198
  159.7 3.1 %collective-permute-start.3 = (bf16[512,2048]{1,0:T(8,128)(2,1)}, bf16[512,2048]{1,0:T(8,128)(2,1)S(1)}, u32[]{:S(2)}, u32[]{:S(2)}) collective-permute-start(bf16[512,2048]{1,0:T(8,128)(2,1)} %projected.1.own_ref), channel_id=1, source_target_pairs={{0,1},{1,0},{2,3},{3,2},{4,5},{5,4},{6,7},{7,6},{8,9},{9,8},{10,11... | collective-permute-start | bytes 6291464 | tf_op jit(solution)/shard_map/ppermute | solution.py:25
  163.6 3.3 %collective-permute-done.3.other_ref = bf16[512,2048]{1,0:T(8,128)(2,1)S(1)} collective-permute-done((bf16[512,2048]{1,0:T(8,128)(2,1)}, bf16[512,2048]{1,0:T(8,128)(2,1)S(1)}, u32[]{:S(2)}, u32[]{:S(2)}) %collective-permute-start.3) | collective-permute-done | bytes 2097184 | tf_op jit(solution)/shard_map/ppermute | solution.py:25
  166.9 11.8 %mixer.1 = (bf16[64,2048]{1,0:T(8,128)(2,1)S(1)}, bf16[256,704]{1,0:T(8,128)(2,1)S(1)}, bf16[256,2048]{1,0:T(8,128)(2,1)S(1)}) custom-call(s32[3]{0:T(128)} %pad_add_fusion.place_ref, bf16[512,2048]{1,0:T(8,128)(2,1)} %projected.1.own_ref, bf16[512,2048]{1,0:T(8,128)(2,1)S(1)} %collective-permute-done.3.other_ref, bf16[8,512,256]{2,1,0:T(8,128)(2,1)} %copy-done.3, ...), custom_call_target="tpu_custom_call" | custom-call | flops 4429185024 | bytes 18874368 | tf_op jit(solution)/shard_map/mixer/pallas_call | solution.py:294
  178.7 2.3 %collective-permute-start.4 = (bf16[256,2048]{1,0:T(8,128)(2,1)S(1)}, bf16[256,2048]{1,0:T(8,128)(2,1)S(1)}, u32[]{:S(2)}, u32[]{:S(2)}) collective-permute-start(bf16[256,2048]{1,0:T(8,128)(2,1)S(1)} %get-tuple-element.15), channel_id=1, source_target_pairs={{0,1},{1,0},{2,3},{3,2},{4,5},{5,4},{6,7},{7,6},{8,9},{9,8},{10,11... | collective-permute-start | bytes 3145736 | tf_op jit(solution)/shard_map/ppermute | solution.py:25
  181.0 2.8 %kept.1 = bf16[256,2048]{1,0:T(8,128)(2,1)S(1)} custom-call(bf16[256,704]{1,0:T(8,128)(2,1)S(1)} %get-tuple-element.14.hidden_ref, bf16[2048,2112]{1,0:T(8,128)(2,1)} %all-gather.2.cloned.1.call-done.ffw_ref), custom_call_target="tpu_custom_call" | custom-call | flops 738197504 | bytes 4194304 | tf_op jit(solution)/shard_map/kept/pallas_call | solution.py:337
  184.2 17.3 %all_to_all.38.pieces_ref = bf16[4,64,2048]{2,1,0:T(8,128)(2,1)S(1)} all-to-all(bf16[4,64,2048]{2,1,0:T(8,128)(2,1)S(1)} %bitcast.20), channel_id=1, replica_groups=mesh['z'=16,'y'=4,'x'=4,'c'=2] {'x'}, dimensions={0} | all-to-all | bytes 2097152 | tf_op jit(solution)/shard_map/all_to_all | solution.py:401
  202.5 10.1 %all_to_all.39 = bf16[8,64,256]{2,1,0:T(8,128)(2,1)S(1)} all-to-all(bf16[8,64,256]{2,1,0:T(8,128)(2,1)S(1)} %last_norm.1), channel_id=1, replica_groups=mesh['z'=16,'y'=4,'x'=4,'c'=2] {'x','c'}, dimensions={0} | all-to-all | bytes 524288 | tf_op jit(solution)/shard_map/all_to_all | solution.py:403
  (43 shorter events, 5.4 us)
Async XLA Ops:
  6.5 13.1 %copy-start.6 = (bf16[128,32]{0,1:T(8,128)(2,1)S(1)}, bf16[128,32]{0,1:T(8,128)(2,1)}, u32[]{:S(2)}) copy-start(bf16[128,32]{0,1:T(8,128)(2,1)} %param.18) | copy-start | bytes 24580
  6.5 13.1 %copy-start.7 = (bf16[32,128]{1,0:T(8,128)(2,1)S(1)}, bf16[32,128]{1,0:T(8,128)(2,1)}, u32[]{:S(2)}) copy-start(bf16[32,128]{1,0:T(8,128)(2,1)} %param.14) | copy-start | bytes 24580
  6.5 13.1 %copy-start.8 = (bf16[32,128]{1,0:T(8,128)(2,1)S(1)}, bf16[32,128]{1,0:T(8,128)(2,1)}, u32[]{:S(2)}) copy-start(bf16[32,128]{1,0:T(8,128)(2,1)} %param.13) | copy-start | bytes 24580
  6.5 160.3 %all-gather.2.cloned.1.call-start = ((), (), s32[]{:S(2)}) async-start(), calls=%async_computation.7 | async-start | bytes 9469952 | tf_op jit(solution)/shard_map/all_gather | solution.py:380
  19.7 47.6 %copy-start.5 = (bf16[512,256]{1,0:T(8,128)(2,1)S(1)}, bf16[512,256]{1,0:T(8,128)(2,1)}, u32[]{:S(2)}) copy-start(bf16[512,256]{1,0:T(8,128)(2,1)} %param.12) | copy-start | bytes 786436
  54.1 0.7 copy-start.4
  68.7 14.5 %slice-start = ((bf16[512,384]{1,0:T(8,128)(2,1)}), bf16[512,128]{1,0:T(8,128)(2,1)S(1)}, s32[]{:S(2)}) async-start(bf16[512,384]{1,0:T(8,128)(2,1)} %copy-done.4), calls=%async_computation.8 | async-start | bytes 262144 | tf_op jit(solution)/shard_map/slice | solution.py:385
  68.7 56.1 %copy-start.9 = (f32[256]{0:T(256)S(1)}, f32[256]{0:T(256)}, u32[]{:S(2)}) copy-start(f32[256]{0:T(256)} %param.23) | copy-start | bytes 3076
  68.7 56.1 %copy-start.10 = (f32[256]{0:T(256)S(1)}, f32[256]{0:T(256)}, u32[]{:S(2)}) copy-start(f32[256]{0:T(256)} %param.19) | copy-start | bytes 3076
  68.7 56.1 %all-to-all-start = ((bf16[8,512,256]{2,1,0:T(8,128)(2,1)}), bf16[8,512,256]{2,1,0:T(8,128)(2,1)S(1)}, u32[]{:S(2)}, u32[]{:S(2)}) async-start(bf16[8,512,256]{2,1,0:T(8,128)(2,1)} %broadcast_in_dim.9), calls=%async_computation | async-start | bytes 4194304 | tf_op jit(solution)/shard_map/all_to_all | solution.py:21
  83.2 55.7 %copy-start = (bf16[1,128,128]{2,1,0:T(8,128)(2,1)S(1)}, bf16[1,128,128]{2,1,0:T(8,128)(2,1)}, u32[]{:S(2)}) copy-start(bf16[1,128,128]{2,1,0:T(8,128)(2,1)} %weight_ref.1) | copy-start | bytes 98308
  83.2 55.7 %copy-start.1 = (f32[128]{0:T(128)S(1)}, f32[128]{0:T(128)}, u32[]{:S(2)}) copy-start(f32[128]{0:T(128)} %param.15) | copy-start | bytes 1540
  83.2 55.7 %copy-start.2 = (f32[1,128]{1,0:T(1,128)S(1)}, f32[1,128]{1,0:T(1,128)}, u32[]{:S(2)}) copy-start(f32[1,128]{1,0:T(1,128)} %bias_ref.1) | copy-start | bytes 1540
  117.0 27.2 %collective-permute-start.2 = (bf16[2048,128]{1,0:T(8,128)(2,1)}, bf16[2048,128]{1,0:T(8,128)(2,1)}, u32[]{:S(2)}, u32[]{:S(2)}) collective-permute-start(bf16[2048,128]{1,0:T(8,128)(2,1)} %all_gather.10), channel_id=1, source_target_pairs={{0,24},{8,0},{16,8},{24,16},{1,25},{9,1},{17,9},{25,17},{2,26},{10... | collective-permute-start | bytes 1572872 | tf_op jit(solution)/shard_map/ppermute | solution.py:351
  119.8 24.4 %collective-permute-start.1 = (bf16[2048,128]{1,0:T(8,128)(2,1)}, bf16[2048,128]{1,0:T(8,128)(2,1)}, u32[]{:S(2)}, u32[]{:S(2)}) collective-permute-start(bf16[2048,128]{1,0:T(8,128)(2,1)} %all_gather.10), channel_id=1, source_target_pairs={{0,16},{8,24},{16,0},{24,8},{1,17},{9,25},{17,1},{25,9},{2,18},{10... | collective-permute-start | bytes 1572872 | tf_op jit(solution)/shard_map/ppermute | solution.py:351
  122.9 25.7 %collective-permute-start = (bf16[2048,128]{1,0:T(8,128)(2,1)}, bf16[2048,128]{1,0:T(8,128)(2,1)}, u32[]{:S(2)}, u32[]{:S(2)}) collective-permute-start(bf16[2048,128]{1,0:T(8,128)(2,1)} %all_gather.10), channel_id=1, source_target_pairs={{0,8},{8,16},{16,24},{24,0},{1,9},{9,17},{17,25},{25,1},{2,10},{10... | collective-permute-start | bytes 1572872 | tf_op jit(solution)/shard_map/ppermute | solution.py:351
  124.9 1.3 copy-start.3
  140.1 12.6 %all-to-all-start.3 = ((bf16[4,512,128]{2,1,0:T(8,128)(2,1)}), bf16[4,512,128]{2,1,0:T(8,128)(2,1)S(1)}, u32[]{:S(2)}, u32[]{:S(2)}) async-start(bf16[4,512,128]{2,1,0:T(8,128)(2,1)} %gated_copies.1), calls=%async_computation.3 | async-start | bytes 1048576 | tf_op jit(solution)/shard_map/all_to_all | solution.py:395
  159.7 7.1 %collective-permute-start.3 = (bf16[512,2048]{1,0:T(8,128)(2,1)}, bf16[512,2048]{1,0:T(8,128)(2,1)S(1)}, u32[]{:S(2)}, u32[]{:S(2)}) collective-permute-start(bf16[512,2048]{1,0:T(8,128)(2,1)} %projected.1.own_ref), channel_id=1, source_target_pairs={{0,1},{1,0},{2,3},{3,2},{4,5},{5,4},{6,7},{7,6},{8,9},{9,8},{10,11... | collective-permute-start | bytes 6291464 | tf_op jit(solution)/shard_map/ppermute | solution.py:25
  178.7 5.1 %collective-permute-start.4 = (bf16[256,2048]{1,0:T(8,128)(2,1)S(1)}, bf16[256,2048]{1,0:T(8,128)(2,1)S(1)}, u32[]{:S(2)}, u32[]{:S(2)}) collective-permute-start(bf16[256,2048]{1,0:T(8,128)(2,1)S(1)} %get-tuple-element.15), channel_id=1, source_target_pairs={{0,1},{1,0},{2,3},{3,2},{4,5},{5,4},{6,7},{7,6},{8,9},{9,8},{10,11... | collective-permute-start | bytes 3145736 | tf_op jit(solution)/shard_map/ppermute | solution.py:25
Sparse Core Ops, SparseCore 0:
  19.7 118.5 all-gather.1
where the time goes:
time: 221 us; the launch traced here: 220 us
  blocking collectives  130 us (59%)
  starting transfers between devices  31.1 us (14%)
  Pallas kernels  26.3 us (12%)
  between operations  13.6 us (6%)
  waiting for transfers between devices  11.8 us (5%)
  local copies, waits for them, and re-layouts  6.04 us (3%)
    all_gather x1, blocking collectives, on_device(): small = lax.all_gather(small, 'z', axis=0, tiled=True)  34.5 us
    all_gather x1, blocking collectives, on_device(): out_x = lax.all_gather(small[:, 2 * sg:], 'x', axis=0, tiled=True)  33.8 us
    all_to_all x2, blocking collectives, sent_to_all(): return lax.all_to_all(copies, axis, split_axis=0, concat_axis=0, tiled=True)  24.3 us
    all_to_all x1, blocking collectives, on_device(): lax.all_to_all(pair.reshape(chips, own_rows, width), 'x', 0, 0, tiled=True)  17.3 us
    all_to_all x1, starting transfers between devices, sent_to_all(): return lax.all_to_all(copies, axis, split_axis=0, concat_axis=0, tiled=True)  14.5 us
    pallas_call x1, Pallas kernels, mixer(): pl.pallas_call(body, out_shape=(pltpu.VMEM((few, width), BF16), pltpu.VME...  11.8 us
    all_to_all x1, blocking collectives, on_device(): known = lax.all_to_all(sums, TP, 0, 0, tiled=True)  10.3 us
    all_to_all x1, blocking collectives, on_device(): return lax.all_to_all(last, TP, 0, 0, tiled=True).reshape(rows, feats)  10.1 us
  transfers between devices with their start and end apart: 8, of which 3 were waited for; matrix products, arithmetic and copies ran while one was open for 1% of the time, Pallas kernels for 6%

commit v1 on v0

--- a/solution.py
+++ b/solution.py
@@ -346,9 +346,9 @@
     )(in_vmem(hidden), in_hbm(ffw))
 
 
-def from_each(value, axis):
+def sent_on(value, axis, steps):
     size = lax.axis_size(axis)
-    return [value] + [lax.ppermute(value, axis, [(i, (i + k) % size) for i in range(size)]) for k in range(1, size)]
+    return lax.ppermute(value, axis, [(i, (i + steps) % size) for i in range(size)])
 
 
 def on_device(
@@ -383,7 +383,9 @@
     small = lax.all_gather(small, "z", axis=0, tiled=True)
     gates = sent_to_all(small[:, : 2 * sg], "y")
     out_x = lax.all_gather(small[:, 2 * sg :], "x", axis=0, tiled=True)
-    out_rows = from_each(out_x, "y")
+    near = [sent_on(out_x, "y", k) for k in (1, 3)]
+    far = sent_on(out_x, "y", 2)
+    out_rows = [out_x, near[0], far, near[1]]
 
     gains = jnp.concatenate([gain_one, gain_two]).reshape(1, rows)
     gated, valued, sums = branches(blocks, gates, gains)

time: 221 us -> 221 us (level)
  no operation moved by 1% of the time
where the time goes in v1:
time: 221 us; the launch traced here: 220 us
  blocking collectives  130 us (59%)
  starting transfers between devices  31.1 us (14%)
  Pallas kernels  26.3 us (12%)
  between operations  13.6 us (6%)
  waiting for transfers between devices  11.8 us (5%)
  local copies, waits for them, and re-layouts  6.04 us (3%)
    all_gather x1, blocking collectives, on_device(): small = lax.all_gather(small, 'z', axis=0, tiled=True)  34.5 us
    all_gather x1, blocking collectives, on_device(): out_x = lax.all_gather(small[:, 2 * sg:], 'x', axis=0, tiled=True)  33.8 us
    all_to_all x2, blocking collectives, sent_to_all(): return lax.all_to_all(copies, axis, split_axis=0, concat_axis=0, tiled=True)  24.3 us
    all_to_all x1, blocking collectives, on_device(): lax.all_to_all(pair.reshape(chips, own_rows, width), 'x', 0, 0, tiled=True)  17.3 us
    all_to_all x1, starting transfers between devices, sent_to_all(): return lax.all_to_all(copies, axis, split_axis=0, concat_axis=0, tiled=True)  14.5 us
    pallas_call x1, Pallas kernels, mixer(): pl.pallas_call(body, out_shape=(pltpu.VMEM((few, width), BF16), pltpu.VME...  11.8 us
    all_to_all x1, blocking collectives, on_device(): known = lax.all_to_all(sums, TP, 0, 0, tiled=True)  10.3 us
    all_to_all x1, blocking collectives, on_device(): return lax.all_to_all(last, TP, 0, 0, tiled=True).reshape(rows, feats)  10.1 us
  transfers between devices with their start and end apart: 8, of which 3 were waited for; matrix products, arithmetic and copies ran while one was open for 1% of the time, Pallas kernels for 6%

profile of v1, /device:TPU:1, one launch (start us, length us, event | category | flops | bytes accessed | tf_op | source)
XLA Modules:
  0.0 220.2 jit_solution(12216790775809021771)
XLA Ops:
  7.6 12.0 %all_to_all.35 = bf16[4,32,2112]{2,1,0:T(8,128)(2,1)} all-to-all(bf16[4,32,2112]{2,1,0:T(8,128)(2,1)S(1)} %broadcast_in_dim.11), channel_id=1, replica_groups=mesh['z'=16,'y'=4,'x'=4,'c'=2] {'y'}, dimensions={0} | all-to-all | bytes 1081344 | tf_op jit(solution)/shard_map/all_to_all | solution.py:21
  19.7 34.5 %all_gather.9 = bf16[512,384]{1,0:T(8,128)(2,1)S(1)} all-gather(bf16[32,384]{1,0:T(8,128)(2,1)S(1)} %pad_maximum_fusion), channel_id=1, replica_groups=mesh['z'=16,'y'=4,'x'=4,'c'=2] {'z'}, dimensions={0}, use_global_device_ids=true | all-gather | bytes 417792 | tf_op jit(solution)/shard_map/all_gather | solution.py:383
  55.0 12.3 %all_to_all.36.gates_ref = bf16[4,512,256]{2,1,0:T(8,128)(2,1)S(1)} all-to-all(bf16[4,512,256]{2,1,0:T(8,128)(2,1)S(1)} %broadcast_in_dim.10), channel_id=1, replica_groups=mesh['z'=16,'y'=4,'x'=4,'c'=2] {'y'}, dimensions={0} | all-to-all | bytes 2097152 | tf_op jit(solution)/shard_map/all_to_all | solution.py:21
  67.3 1.5 broadcast_in_dim.9
  68.7 14.5 %all-to-all-start = ((bf16[8,512,256]{2,1,0:T(8,128)(2,1)}), bf16[8,512,256]{2,1,0:T(8,128)(2,1)S(1)}, u32[]{:S(2)}, u32[]{:S(2)}) async-start(bf16[8,512,256]{2,1,0:T(8,128)(2,1)} %broadcast_in_dim.9), calls=%async_computation | async-start | bytes 4194304 | tf_op jit(solution)/shard_map/all_to_all | solution.py:21
  83.2 33.8 %all_gather.10 = bf16[2048,128]{1,0:T(8,128)(2,1)} all-gather(bf16[512,128]{1,0:T(8,128)(2,1)S(1)} %slice-done), channel_id=1, replica_groups=mesh['z'=16,'y'=4,'x'=4,'c'=2] {'x'}, dimensions={0}, use_global_device_ids=true | all-gather | bytes 655360 | tf_op jit(solution)/shard_map/all_gather | solution.py:385
  117.0 2.8 %collective-permute-start.2 = (bf16[2048,128]{1,0:T(8,128)(2,1)}, bf16[2048,128]{1,0:T(8,128)(2,1)}, u32[]{:S(2)}, u32[]{:S(2)}) collective-permute-start(bf16[2048,128]{1,0:T(8,128)(2,1)} %all_gather.10), channel_id=1, source_target_pairs={{0,24},{8,0},{16,8},{24,16},{1,25},{9,1},{17,9},{25,17},{2,26},{10... | collective-permute-start | bytes 1572872 | tf_op jit(solution)/shard_map/ppermute | solution.py:351
  119.8 3.1 %collective-permute-start.1 = (bf16[2048,128]{1,0:T(8,128)(2,1)}, bf16[2048,128]{1,0:T(8,128)(2,1)}, u32[]{:S(2)}, u32[]{:S(2)}) collective-permute-start(bf16[2048,128]{1,0:T(8,128)(2,1)} %all_gather.10), channel_id=1, source_target_pairs={{0,16},{8,24},{16,0},{24,8},{1,17},{9,25},{17,1},{25,9},{2,18},{10... | collective-permute-start | bytes 1572872 | tf_op jit(solution)/shard_map/ppermute | solution.py:351
  122.9 1.9 collective-permute-start
  124.9 1.3 copy-done.3
  126.2 2.5 %branches.1 = (f32[512,128]{1,0:T(8,128)S(1)}, f32[512,128]{1,0:T(8,128)S(1)}, f32[8,4,512]{2,1,0:T(4,128)S(1)}) custom-call(bf16[8,512,256]{2,1,0:T(8,128)(2,1)} %copy-done.3, bf16[4,512,256]{2,1,0:T(8,128)(2,1)S(1)} %all_to_all.36.gates_ref, f32[1,512]{1,0:T(1,128)S(1)} %bitcast.18), custom_call_target="tpu_custom_call" | custom-call | flops 536870912 | bytes 4194304 | tf_op jit(solution)/shard_map/branches/pallas_call | solution.py:99
  128.6 10.3 %all_to_all.37.known_ref = f32[8,4,512]{2,1,0:T(4,128)S(1)} all-to-all(f32[8,4,512]{2,1,0:T(4,128)S(1)} %get-tuple-element.11), channel_id=1, replica_groups=mesh['z'=16,'y'=4,'x'=4,'c'=2] {'x','c'}, dimensions={0} | all-to-all | bytes 131072 | tf_op jit(solution)/shard_map/all_to_all | solution.py:392
  138.9 1.2 gated_copies.1
  140.1 3.5 %all-to-all-start.3 = ((bf16[4,512,128]{2,1,0:T(8,128)(2,1)}), bf16[4,512,128]{2,1,0:T(8,128)(2,1)S(1)}, u32[]{:S(2)}, u32[]{:S(2)}) async-start(bf16[4,512,128]{2,1,0:T(8,128)(2,1)} %gated_copies.1), calls=%async_computation.3 | async-start | bytes 1048576 | tf_op jit(solution)/shard_map/all_to_all | solution.py:397
  144.2 4.4 %collective-permute-done = bf16[2048,128]{1,0:T(8,128)(2,1)} collective-permute-done((bf16[2048,128]{1,0:T(8,128)(2,1)}, bf16[2048,128]{1,0:T(8,128)(2,1)}, u32[]{:S(2)}, u32[]{:S(2)}) %collective-permute-start) | collective-permute-done | bytes 524320 | tf_op jit(solution)/shard_map/ppermute | solution.py:351
  148.6 4.2 %all-to-all-done.3.gated_ref = bf16[4,512,128]{2,1,0:T(8,128)(2,1)S(1)} async-done(((bf16[4,512,128]{2,1,0:T(8,128)(2,1)}), bf16[4,512,128]{2,1,0:T(8,128)(2,1)S(1)}, u32[]{:S(2)}, u32[]{:S(2)}) %all-to-all-start.3) | async-done | bytes 524320 | tf_op jit(solution)/shard_map/all_to_all | solution.py:397
  152.7 7.0 %projected.1.own_ref = bf16[512,2048]{1,0:T(8,128)(2,1)} custom-call(s32[3]{0:T(128)} %pad_add_fusion.place_ref, bf16[4,512,128]{2,1,0:T(8,128)(2,1)S(1)} %all-to-all-done.3.gated_ref, bf16[4,16,32,128]{3,2,1,0:T(8,128)(2,1)} %bitcast.6.rest_0_, bf16[4,16,32,128]{3,2,1,0:T(8,128)(2,1)} %bitcast.7.rest_1_, bf16[4,16,32,128]{3,2,1,0:T(8,128)(2,1)} %bitcast.8.rest_2_, ...), custom_call_target="tpu_custom_call" | custom-call | flops 1073741824 | bytes 6291456 | tf_op jit(solution)/shard_map/projected/pallas_call | solution.py:198
  159.7 3.1 %collective-permute-start.3 = (bf16[512,2048]{1,0:T(8,128)(2,1)}, bf16[512,2048]{1,0:T(8,128)(2,1)S(1)}, u32[]{:S(2)}, u32[]{:S(2)}) collective-permute-start(bf16[512,2048]{1,0:T(8,128)(2,1)} %projected.1.own_ref), channel_id=1, source_target_pairs={{0,1},{1,0},{2,3},{3,2},{4,5},{5,4},{6,7},{7,6},{8,9},{9,8},{10,11... | collective-permute-start | bytes 6291464 | tf_op jit(solution)/shard_map/ppermute | solution.py:25
  163.6 3.3 %collective-permute-done.3.other_ref = bf16[512,2048]{1,0:T(8,128)(2,1)S(1)} collective-permute-done((bf16[512,2048]{1,0:T(8,128)(2,1)}, bf16[512,2048]{1,0:T(8,128)(2,1)S(1)}, u32[]{:S(2)}, u32[]{:S(2)}) %collective-permute-start.3) | collective-permute-done | bytes 2097184 | tf_op jit(solution)/shard_map/ppermute | solution.py:25
  166.9 11.8 %mixer.1 = (bf16[64,2048]{1,0:T(8,128)(2,1)S(1)}, bf16[256,704]{1,0:T(8,128)(2,1)S(1)}, bf16[256,2048]{1,0:T(8,128)(2,1)S(1)}) custom-call(s32[3]{0:T(128)} %pad_add_fusion.place_ref, bf16[512,2048]{1,0:T(8,128)(2,1)} %projected.1.own_ref, bf16[512,2048]{1,0:T(8,128)(2,1)S(1)} %collective-permute-done.3.other_ref, bf16[8,512,256]{2,1,0:T(8,128)(2,1)} %copy-done.3, ...), custom_call_target="tpu_custom_call" | custom-call | flops 4429185024 | bytes 18874368 | tf_op jit(solution)/shard_map/mixer/pallas_call | solution.py:294
  178.7 2.3 %collective-permute-start.4 = (bf16[256,2048]{1,0:T(8,128)(2,1)S(1)}, bf16[256,2048]{1,0:T(8,128)(2,1)S(1)}, u32[]{:S(2)}, u32[]{:S(2)}) collective-permute-start(bf16[256,2048]{1,0:T(8,128)(2,1)S(1)} %get-tuple-element.15), channel_id=1, source_target_pairs={{0,1},{1,0},{2,3},{3,2},{4,5},{5,4},{6,7},{7,6},{8,9},{9,8},{10,11... | collective-permute-start | bytes 3145736 | tf_op jit(solution)/shard_map/ppermute | solution.py:25
  181.0 2.8 %kept.1 = bf16[256,2048]{1,0:T(8,128)(2,1)S(1)} custom-call(bf16[256,704]{1,0:T(8,128)(2,1)S(1)} %get-tuple-element.14.hidden_ref, bf16[2048,2112]{1,0:T(8,128)(2,1)} %all-gather.2.cloned.1.call-done.ffw_ref), custom_call_target="tpu_custom_call" | custom-call | flops 738197504 | bytes 4194304 | tf_op jit(solution)/shard_map/kept/pallas_call | solution.py:337
  184.2 17.3 %all_to_all.38.pieces_ref = bf16[4,64,2048]{2,1,0:T(8,128)(2,1)S(1)} all-to-all(bf16[4,64,2048]{2,1,0:T(8,128)(2,1)S(1)} %bitcast.20), channel_id=1, replica_groups=mesh['z'=16,'y'=4,'x'=4,'c'=2] {'x'}, dimensions={0} | all-to-all | bytes 2097152 | tf_op jit(solution)/shard_map/all_to_all | solution.py:403
  202.5 10.1 %all_to_all.39 = bf16[8,64,256]{2,1,0:T(8,128)(2,1)S(1)} all-to-all(bf16[8,64,256]{2,1,0:T(8,128)(2,1)S(1)} %last_norm.1), channel_id=1, replica_groups=mesh['z'=16,'y'=4,'x'=4,'c'=2] {'x','c'}, dimensions={0} | all-to-all | bytes 524288 | tf_op jit(solution)/shard_map/all_to_all | solution.py:405
  (43 shorter events, 5.4 us)
Async XLA Ops:
  6.5 13.1 %copy-start.6 = (bf16[128,32]{0,1:T(8,128)(2,1)S(1)}, bf16[128,32]{0,1:T(8,128)(2,1)}, u32[]{:S(2)}) copy-start(bf16[128,32]{0,1:T(8,128)(2,1)} %param.18) | copy-start | bytes 24580
  6.5 13.1 %copy-start.7 = (bf16[32,128]{1,0:T(8,128)(2,1)S(1)}, bf16[32,128]{1,0:T(8,128)(2,1)}, u32[]{:S(2)}) copy-start(bf16[32,128]{1,0:T(8,128)(2,1)} %param.14) | copy-start | bytes 24580
  6.5 13.1 %copy-start.8 = (bf16[32,128]{1,0:T(8,128)(2,1)S(1)}, bf16[32,128]{1,0:T(8,128)(2,1)}, u32[]{:S(2)}) copy-start(bf16[32,128]{1,0:T(8,128)(2,1)} %param.13) | copy-start | bytes 24580
  6.5 160.3 %all-gather.2.cloned.1.call-start = ((), (), s32[]{:S(2)}) async-start(), calls=%async_computation.7 | async-start | bytes 9469952 | tf_op jit(solution)/shard_map/all_gather | solution.py:380
  19.7 47.6 %copy-start.5 = (bf16[512,256]{1,0:T(8,128)(2,1)S(1)}, bf16[512,256]{1,0:T(8,128)(2,1)}, u32[]{:S(2)}) copy-start(bf16[512,256]{1,0:T(8,128)(2,1)} %param.12) | copy-start | bytes 786436
  54.1 0.7 copy-start.4
  68.7 14.5 %slice-start = ((bf16[512,384]{1,0:T(8,128)(2,1)}), bf16[512,128]{1,0:T(8,128)(2,1)S(1)}, s32[]{:S(2)}) async-start(bf16[512,384]{1,0:T(8,128)(2,1)} %copy-done.4), calls=%async_computation.8 | async-start | bytes 262144 | tf_op jit(solution)/shard_map/slice | solution.py:385
  68.7 56.1 %copy-start.9 = (f32[256]{0:T(256)S(1)}, f32[256]{0:T(256)}, u32[]{:S(2)}) copy-start(f32[256]{0:T(256)} %param.23) | copy-start | bytes 3076
  68.7 56.1 %copy-start.10 = (f32[256]{0:T(256)S(1)}, f32[256]{0:T(256)}, u32[]{:S(2)}) copy-start(f32[256]{0:T(256)} %param.19) | copy-start | bytes 3076
  68.7 56.1 %all-to-all-start = ((bf16[8,512,256]{2,1,0:T(8,128)(2,1)}), bf16[8,512,256]{2,1,0:T(8,128)(2,1)S(1)}, u32[]{:S(2)}, u32[]{:S(2)}) async-start(bf16[8,512,256]{2,1,0:T(8,128)(2,1)} %broadcast_in_dim.9), calls=%async_computation | async-start | bytes 4194304 | tf_op jit(solution)/shard_map/all_to_all | solution.py:21
  83.2 55.7 %copy-start = (bf16[1,128,128]{2,1,0:T(8,128)(2,1)S(1)}, bf16[1,128,128]{2,1,0:T(8,128)(2,1)}, u32[]{:S(2)}) copy-start(bf16[1,128,128]{2,1,0:T(8,128)(2,1)} %weight_ref.1) | copy-start | bytes 98308
  83.2 55.7 %copy-start.1 = (f32[128]{0:T(128)S(1)}, f32[128]{0:T(128)}, u32[]{:S(2)}) copy-start(f32[128]{0:T(128)} %param.15) | copy-start | bytes 1540
  83.2 55.7 %copy-start.2 = (f32[1,128]{1,0:T(1,128)S(1)}, f32[1,128]{1,0:T(1,128)}, u32[]{:S(2)}) copy-start(f32[1,128]{1,0:T(1,128)} %bias_ref.1) | copy-start | bytes 1540
  117.0 27.2 %collective-permute-start.2 = (bf16[2048,128]{1,0:T(8,128)(2,1)}, bf16[2048,128]{1,0:T(8,128)(2,1)}, u32[]{:S(2)}, u32[]{:S(2)}) collective-permute-start(bf16[2048,128]{1,0:T(8,128)(2,1)} %all_gather.10), channel_id=1, source_target_pairs={{0,24},{8,0},{16,8},{24,16},{1,25},{9,1},{17,9},{25,17},{2,26},{10... | collective-permute-start | bytes 1572872 | tf_op jit(solution)/shard_map/ppermute | solution.py:351
  119.8 24.4 %collective-permute-start.1 = (bf16[2048,128]{1,0:T(8,128)(2,1)}, bf16[2048,128]{1,0:T(8,128)(2,1)}, u32[]{:S(2)}, u32[]{:S(2)}) collective-permute-start(bf16[2048,128]{1,0:T(8,128)(2,1)} %all_gather.10), channel_id=1, source_target_pairs={{0,16},{8,24},{16,0},{24,8},{1,17},{9,25},{17,1},{25,9},{2,18},{10... | collective-permute-start | bytes 1572872 | tf_op jit(solution)/shard_map/ppermute | solution.py:351
  122.9 25.7 %collective-permute-start = (bf16[2048,128]{1,0:T(8,128)(2,1)}, bf16[2048,128]{1,0:T(8,128)(2,1)}, u32[]{:S(2)}, u32[]{:S(2)}) collective-permute-start(bf16[2048,128]{1,0:T(8,128)(2,1)} %all_gather.10), channel_id=1, source_target_pairs={{0,8},{8,16},{16,24},{24,0},{1,9},{9,17},{17,25},{25,1},{2,10},{10... | collective-permute-start | bytes 1572872 | tf_op jit(solution)/shard_map/ppermute | solution.py:351
  124.9 1.3 copy-start.3
  140.1 12.6 %all-to-all-start.3 = ((bf16[4,512,128]{2,1,0:T(8,128)(2,1)}), bf16[4,512,128]{2,1,0:T(8,128)(2,1)S(1)}, u32[]{:S(2)}, u32[]{:S(2)}) async-start(bf16[4,512,128]{2,1,0:T(8,128)(2,1)} %gated_copies.1), calls=%async_computation.3 | async-start | bytes 1048576 | tf_op jit(solution)/shard_map/all_to_all | solution.py:397
  159.7 7.1 %collective-permute-start.3 = (bf16[512,2048]{1,0:T(8,128)(2,1)}, bf16[512,2048]{1,0:T(8,128)(2,1)S(1)}, u32[]{:S(2)}, u32[]{:S(2)}) collective-permute-start(bf16[512,2048]{1,0:T(8,128)(2,1)} %projected.1.own_ref), channel_id=1, source_target_pairs={{0,1},{1,0},{2,3},{3,2},{4,5},{5,4},{6,7},{7,6},{8,9},{9,8},{10,11... | collective-permute-start | bytes 6291464 | tf_op jit(solution)/shard_map/ppermute | solution.py:25
  178.7 5.1 %collective-permute-start.4 = (bf16[256,2048]{1,0:T(8,128)(2,1)S(1)}, bf16[256,2048]{1,0:T(8,128)(2,1)S(1)}, u32[]{:S(2)}, u32[]{:S(2)}) collective-permute-start(bf16[256,2048]{1,0:T(8,128)(2,1)S(1)} %get-tuple-element.15), channel_id=1, source_target_pairs={{0,1},{1,0},{2,3},{3,2},{4,5},{5,4},{6,7},{7,6},{8,9},{9,8},{10,11... | collective-permute-start | bytes 3145736 | tf_op jit(solution)/shard_map/ppermute | solution.py:25
Sparse Core Ops, SparseCore 0:
  19.7 118.5 all-gather.1
